TPU v7x, 32 devices: a whole 2x2x4 slice. The times are simulated.
32 devices in a mesh: fs: 8 (over z, y), tp: 4 (over x, core).
Axes of the slice: x: 2, y: 2, z: 4, core: 2. Of those that a mesh axis runs over, the one named last changes fastest.
Arguments:
- layer_input: bfloat16 [20480, 4096], P('fs'), may hold values from -140 to 140
- query_cotangent: bfloat16 [20480, 2048], P('fs', 'tp'), may hold values from -0.46817673 to 0.46817673
- value_cotangent: bfloat16 [20480, 512], P('fs', 'tp'), may hold values from -0.46817673 to 0.46817673
- query_weight: float32 [4096, 2048], P('fs', 'tp'), may hold values from -0.09375 to 0.09375
- value_weight: float32 [4096, 512], P('fs', 'tp'), may hold values from -0.09375 to 0.09375
- query_moment: float32 [4096, 2048], P('fs', 'tp'), may hold values from -18 to 18
- value_moment: float32 [4096, 512], P('fs', 'tp'), may hold values from -18 to 18
- query_left_stat: float32 [16, 256, 256], P('fs'), may hold values from -24 to 24
- value_left_stat: float32 [16, 256, 256], P('fs'), may hold values from -24 to 24
- query_right_stat: float32 [32, 64, 64], P('tp'), may hold values from -24 to 24
- value_right_stat: float32 [8, 64, 64], P('tp'), may hold values from -24 to 24
- query_left_root: bfloat16 [16, 256, 256], P('fs'), may hold values from -1.5 to 2
- value_left_root: bfloat16 [16, 256, 256], P('fs'), may hold values from -1.5 to 2
- query_right_root: bfloat16 [32, 64, 64], P('tp'), may hold values from -1.5 to 2
- value_right_root: bfloat16 [8, 64, 64], P('tp'), may hold values from -1.5 to 2
Outputs:
- query_update: float32 [4096, 2048], P('fs', 'tp')
- value_update: float32 [4096, 512], P('fs', 'tp')
- query_moment_new: float32 [4096, 2048], P('fs', 'tp')
- value_moment_new: float32 [4096, 512], P('fs', 'tp')
- query_left_new: float32 [16, 256, 256], P('fs')
- value_left_new: float32 [16, 256, 256], P('fs')
- query_right_new: float32 [32, 64, 64], P('tp')
- value_right_new: float32 [8, 64, 64], P('tp')
- query_copy: bfloat16 [4096, 2048], P(None, 'tp')
- value_copy: bfloat16 [4096, 512], P(None, 'tp')
All inputs are finite; a program needn't handle non-finite values.
Results may differ from a plain program's by a relative error of at most 0.0075.
Values may be sent and summed in bfloat16 or wider, within the bound.
A program may use at most 128 MiB of HBM per device.

v0:
```python
import jax
import jax.numpy as jnp
from jax import lax
from jax.sharding import PartitionSpec as P

D = 4096
HEAD = 64
BLOCK = 256
Q_COLS = 2048
V_COLS = 512


momentum_decay = 0.9
statistic_decay = 0.9
learning_rate = 0.002
epsilon = 1e-06
highest = lax.Precision.HIGHEST


def token_sum(inputs, cotangent):
    return lax.dot_general(
        inputs, cotangent, (((0,), (0,)), ((), ())), preferred_element_type=jnp.float32
    )


def precondition(moment, left_root, right_root):
    shard_rows, columns = moment.shape
    head_count = columns // HEAD
    by_head = jnp.einsum(
        "rhk,hkl->rhl",
        moment.reshape(shard_rows, head_count, HEAD),
        right_root.astype(jnp.float32),
        precision=highest,
    )
    by_block = by_head.reshape(shard_rows // BLOCK, BLOCK, columns)
    return jnp.einsum(
        "bij,bjc->bic", left_root.astype(jnp.float32), by_block, precision=highest
    ).reshape(shard_rows, columns)


def local_terms(gradient, moment, left_root, right_root):
    shard_rows, columns = gradient.shape
    moment_new = momentum_decay * moment + (1.0 - momentum_decay) * gradient
    blocks = gradient.reshape(shard_rows // BLOCK, BLOCK, columns)
    left_part = jnp.einsum("bic,bjc->bij", blocks, blocks, precision=highest)
    per_head = gradient.reshape(shard_rows, columns // HEAD, HEAD)
    right_part = jnp.einsum("rhk,rhl->hkl", per_head, per_head, precision=highest)
    direction = precondition(moment_new, left_root, right_root)
    squares = jnp.stack([jnp.sum(moment_new * moment_new), jnp.sum(direction * direction)])
    return (moment_new, left_part, right_part, direction, squares)


def local(
    layer_input,
    query_cotangent,
    value_cotangent,
    query_weight,
    value_weight,
    query_moment,
    value_moment,
    query_left_stat,
    value_left_stat,
    query_right_stat,
    value_right_stat,
    query_left_root,
    value_left_root,
    query_right_root,
    value_right_root,
):
    query_width = query_cotangent.shape[1]
    both_cotangents = jnp.concatenate([query_cotangent, value_cotangent], axis=1)
    both_gradients = lax.psum_scatter(
        token_sum(layer_input, both_cotangents), "fs", scatter_dimension=0, tiled=True
    )
    query_gradient = both_gradients[:, :query_width]
    value_gradient = both_gradients[:, query_width:]
    query_moment_new, query_left_part, query_right_part, query_direction, query_squares = (
        local_terms(query_gradient, query_moment, query_left_root, query_right_root)
    )
    value_moment_new, value_left_part, value_right_part, value_direction, value_squares = (
        local_terms(value_gradient, value_moment, value_left_root, value_right_root)
    )
    squares = jnp.concatenate([query_squares, value_squares])
    query_right_sum, value_right_sum = (
        lax.psum(query_right_part.astype(jnp.bfloat16), "fs").astype(jnp.float32),
        lax.psum(value_right_part.astype(jnp.bfloat16), "fs").astype(jnp.float32),
    )
    query_left_sum, value_left_sum = (
        lax.psum(query_left_part.astype(jnp.bfloat16), "tp").astype(jnp.float32),
        lax.psum(value_left_part.astype(jnp.bfloat16), "tp").astype(jnp.float32),
    )
    all_squares = lax.psum(squares, ("fs", "tp"))
    query_left_new = (
        statistic_decay * query_left_stat + (1.0 - statistic_decay) / Q_COLS * query_left_sum
    )
    value_left_new = (
        statistic_decay * value_left_stat + (1.0 - statistic_decay) / V_COLS * value_left_sum
    )
    query_right_new = (
        statistic_decay * query_right_stat + (1.0 - statistic_decay) / D * query_right_sum
    )
    value_right_new = (
        statistic_decay * value_right_stat + (1.0 - statistic_decay) / D * value_right_sum
    )
    query_update = jnp.sqrt(all_squares[0] / (all_squares[1] + epsilon)) * query_direction
    value_update = jnp.sqrt(all_squares[2] / (all_squares[3] + epsilon)) * value_direction
    query_shard = (query_weight - learning_rate * query_update).astype(jnp.bfloat16)
    value_shard = (value_weight - learning_rate * value_update).astype(jnp.bfloat16)
    query_copy, value_copy = (
        lax.all_gather(query_shard, "fs", axis=0, tiled=True),
        lax.all_gather(value_shard, "fs", axis=0, tiled=True),
    )
    return (
        query_update,
        value_update,
        query_moment_new,
        value_moment_new,
        query_left_new,
        value_left_new,
        query_right_new,
        value_right_new,
        query_copy,
        value_copy,
    )


def solution(mesh):
    placed = (
        P("fs", None),
        P("fs", "tp"),
        P("fs", "tp"),
        P("fs", "tp"),
        P("fs", "tp"),
        P("fs", "tp"),
        P("fs", "tp"),
        P("fs", None, None),
        P("fs", None, None),
        P("tp", None, None),
        P("tp", None, None),
        P("fs", None, None),
        P("fs", None, None),
        P("tp", None, None),
        P("tp", None, None),
    )
    return jax.shard_map(
        local,
        mesh=mesh,
        in_specs=placed,
        out_specs=(
            P("fs", "tp"),
            P("fs", "tp"),
            P("fs", "tp"),
            P("fs", "tp"),
            P("fs", None, None),
            P("fs", None, None),
            P("tp", None, None),
            P("tp", None, None),
            P(None, "tp"),
            P(None, "tp"),
        ),
        check_vma=False,
    )
```

profile of v0, /device:TPU:0, one launch (start us, length us, event | category | flops | bytes accessed | tf_op | source)
XLA Modules:
  0.0 512.9 jit_solution(3195955658530197964)
XLA Ops:
  7.2 0.0 reduce-scatter.2.cloned.1.call-start
  7.2 21.4 %convolution_bitcast_fusion = f32[4096,640]{0,1:T(8,128)} fusion(bf16[2560,4096]{1,0:T(8,128)(2,1)} %param.15, bf16[2560,128]{1,0:T(8,128)(2,1)} %param.17, bf16[2560,512]{1,0:T(8,128)(2,1)} %param.16), kind=kOutput, calls=%fused_computation | convolution fusion | flops 13428326400 | bytes 34734080 | tf_op jit(solution)/shard_map/dot_general | solution.py:21
  28.6 0.0 all-reduce.4.cloned.1.call-start
  28.7 1.1 copy-done.4
  29.8 0.3 copy.37
  30.2 0.8 copy.40
  31.0 179.1 %reduce-scatter.2.cloned.1.call-done = f32[512,640]{0,1:T(8,128)} async-done(((f32[4096,640]{0,1:T(8,128)}), f32[512,640]{0,1:T(8,128)}) %reduce-scatter.2.cloned.1.call-update) | async-done | bytes 1310736 | tf_op jit(solution)/shard_map/reduce_scatter | solution.py:72
  210.1 2.2 multiply_reduce_fusion.1
  212.3 1.6 convolution_bitcast_fusion.1
  213.9 1.9 reshape.59
  215.8 2.4 multiply_reduce_fusion.3
  218.2 0.7 copy-done.3
  218.9 1.8 convolution_bitcast_fusion.2
  220.7 1.8 reshape.61
  222.5 2.3 multiply_reduce_fusion
  224.8 2.7 multiply_reduce_fusion.2
  227.5 2.7 pad_maximum_fusion
  230.2 39.4 %psum.35 = f32[4]{0:T(128)S(1)} all-reduce(f32[4]{0:T(128)S(1)} %pad_maximum_fusion), channel_id=1, replica_groups=mesh['fs'=8,'tp'=4] {'fs','tp'}, use_global_device_ids=true, to_apply=%region_5.0 | all-reduce | flops 4 | bytes 32 | tf_op jit(solution)/shard_map/psum | solution.py:92
  269.6 0.3 copy.52
  270.0 1.9 convolution_convert_fusion
  271.8 1.9 copy.53
  273.7 2.3 convolution_convert_fusion.1
  276.0 1.7 convolution_convert_fusion.2
  277.7 0.0 all-reduce.4.cloned.1.call-update
  277.8 0.0 all-reduce.6.cloned.1.call-start
  277.8 0.6 fusion.8
  279.8 0.0 all-reduce.6.cloned.1.call-update
  279.8 0.0 all-gather.5.cloned.1.call-start
  279.8 1.0 multiply_bitcast_fusion
  280.8 0.1 copy.43
  280.9 1.7 subtract_convert_fusion.1
  282.7 0.0 all-gather.5.cloned.1.call-update
  282.7 0.0 all-gather.3.cloned.1.call-start
  284.1 0.1 broadcast_multiply_fusion
  284.3 2.6 subtract_convert_fusion
  286.8 1.3 copy.48
  288.2 1.8 copy.49
  289.9 1.5 convolution_convert_fusion.3
  291.4 36.9 %psum.39 = bf16[2,64,64]{2,1,0:T(8,128)(2,1)S(1)} all-reduce(bf16[2,64,64]{2,1,0:T(8,128)(2,1)S(1)} %convolution_convert_fusion.3), channel_id=1, replica_groups=mesh['fs'=8,'tp'=4] {'fs'}, use_global_device_ids=true, to_apply=%region_9.0 | all-reduce | flops 8192 | bytes 32768 | tf_op jit(solution)/shard_map/psum | solution.py:86
  328.3 0.6 multiply_add_fusion.5
  329.0 19.2 %all-reduce.4.cloned.1.call-done = bf16[8,64,64]{2,1,0:T(8,128)(2,1)} async-done(((bf16[8,64,64]{2,1,0:T(8,128)(2,1)}), bf16[8,64,64]{2,1,0:T(8,128)(2,1)}) %all-reduce.4.cloned.1.call-update) | async-done | bytes 65552 | tf_op jit(solution)/shard_map/psum | solution.py:85
  348.1 1.8 multiply_add_fusion.3
  349.9 34.4 %all-reduce.6.cloned.1.call-done = (bf16[2,256,256]{2,1,0:T(8,128)(2,1)}, bf16[2,256,256]{2,1,0:T(8,128)(2,1)}) async-done(((bf16[2,256,256]{2,1,0:T(8,128)(2,1)}, bf16[2,256,256]{2,1,0:T(8,128)(2,1)}), (bf16[2,256,256]{2,1,0:T(8,128)(2,1)}, bf16[2,256,256]{2,1,0:T(8,128)(2,1)})) %all-reduce.6.cloned.1.call-update) | async-done | bytes 524304 | tf_op jit(solution)/shard_map/psum | solution.py:89
  384.3 2.2 multiply_add_fusion.1
  386.5 40.3 %all-gather.5.cloned.1.call-done = bf16[4096,128]{1,0:T(8,128)(2,1)} async-done(((bf16[512,128]{1,0:T(8,128)(2,1)}), bf16[4096,128]{1,0:T(8,128)(2,1)}) %all-gather.5.cloned.1.call-update) | async-done | bytes 1048592 | tf_op jit(solution)/shard_map/all_gather | solution.py:111
  426.7 74.1 %all-gather.3.cloned.1.call-done = bf16[4096,512]{1,0:T(8,128)(2,1)} async-done(((bf16[512,512]{1,0:T(8,128)(2,1)}), bf16[4096,512]{1,0:T(8,128)(2,1)}) %all-gather.3.cloned.1.call-update) | async-done | bytes 4194320 | tf_op jit(solution)/shard_map/all_gather | solution.py:110
  500.8 4.6 copy.67
  505.4 1.0 copy.68
  (24 shorter events, 0.1 us)
Async XLA Ops:
  7.2 215.3 %copy-start = (bf16[2,256,256]{2,1,0:T(8,128)(2,1)S(1)}, bf16[2,256,256]{2,1,0:T(8,128)(2,1)}, u32[]{:S(2)}) copy-start(bf16[2,256,256]{2,1,0:T(8,128)(2,1)} %param.26) | copy-start | bytes 786436
  7.2 202.9 %reduce-scatter.2.cloned.1.call-start = ((), (), s32[]{:S(2)}) async-start(), calls=%async_computation.1 | async-start | bytes 11796480 | tf_op jit(solution)/shard_map/reduce_scatter | solution.py:72
  28.6 1.2 copy-start.4
  28.6 1.6 copy-start.9
  28.6 183.7 %copy-start.10 = (bf16[8,64,64]{2,1,0:T(8,128)(2,1)S(1)}, bf16[8,64,64]{2,1,0:T(8,128)(2,1)}, u32[]{:S(2)}) copy-start(bf16[8,64,64]{2,1,0:T(8,128)(2,1)} %param.28) | copy-start | bytes 196612
  28.6 319.5 %all-reduce.4.cloned.1.call-start = ((), (), s32[]{:S(2)}) async-start(), calls=%async_computation.2 | async-start | bytes 262144 | tf_op jit(solution)/shard_map/psum | solution.py:85
  218.2 0.7 copy-start.3
  271.8 12.3 %copy-start.1 = (f32[2,512,256]{1,2,0:T(8,128)S(1)}, f32[2,512,256]{1,2,0:T(8,128)}, u32[]{:S(2)}) copy-start(f32[2,512,256]{1,2,0:T(8,128)} %get-tuple-element.45) | copy-start | bytes 3145732
  277.8 106.6 %all-reduce.6.cloned.1.call-start = ((), (), s32[]{:S(2)}) async-start(), calls=%async_computation.5 | async-start | bytes 1048576 | tf_op jit(solution)/shard_map/psum | solution.py:89
  279.8 147.0 %all-gather.5.cloned.1.call-start = ((), (), s32[]{:S(2)}) async-start(), calls=%async_computation.4 | async-start | bytes 1179648 | tf_op jit(solution)/shard_map/all_gather | solution.py:111
  280.9 3.2 copy-start.6
  282.7 218.1 %all-gather.3.cloned.1.call-start = ((), (), s32[]{:S(2)}) async-start(), calls=%async_computation.3 | async-start | bytes 4718592 | tf_op jit(solution)/shard_map/all_gather | solution.py:110
  284.1 44.2 %copy-start.11 = (f32[2,64,64]{2,1,0:T(8,128)S(1)}, f32[2,64,64]{2,1,0:T(8,128)}, u32[]{:S(2)}) copy-start(f32[2,64,64]{2,1,0:T(8,128)} %param.25) | copy-start | bytes 98308
  284.2 102.3 %copy-start.2 = (f32[2,512,256]{1,2,0:T(8,128)}, f32[2,512,256]{1,2,0:T(8,128)S(1)}, u32[]{:S(2)}) copy-start(f32[2,512,256]{1,2,0:T(8,128)S(1)} %broadcast_multiply_fusion) | copy-start | bytes 3145732
  284.2 100.1 %copy-start.7 = (f32[2,256,256]{2,1,0:T(8,128)S(1)}, f32[2,256,256]{2,1,0:T(8,128)}, u32[]{:S(2)}) copy-start(f32[2,256,256]{2,1,0:T(8,128)} %param.23) | copy-start | bytes 1572868
  284.2 100.1 %copy-start.8 = (f32[2,256,256]{2,1,0:T(8,128)S(1)}, f32[2,256,256]{2,1,0:T(8,128)}, u32[]{:S(2)}) copy-start(f32[2,256,256]{2,1,0:T(8,128)} %param.22) | copy-start | bytes 1572868
  500.8 4.6 copy-start.5
Sparse Core Ops, SparseCore 0:
  28.8 181.3 reduce-scatter.1
  277.9 70.1 all-reduce.3
  351.7 32.5 all-reduce.5
  386.3 40.3 all-gather.4
  429.3 71.4 all-gather.2
where the time goes:
time: 514 us; the launch traced here: 513 us
  waiting for transfers between devices  347 us (68%)
  blocking collectives  76.3 us (15%)
  matrix products  37.1 us (7%)
  local copies, waits for them, and re-layouts  18.3 us (4%)
  other arithmetic  17.2 us (3%)
  between operations  16.6 us (3%)
    reduce_scatter x1, waiting for transfers between devices, local(): lax.psum_scatter(token_sum(layer_input, both_cotangents), 'fs', scatter_d...  179 us
    all_gather x1, waiting for transfers between devices, local(): lax.all_gather(query_shard, 'fs', axis=0, tiled=True)  74.1 us
    all_gather x1, waiting for transfers between devices, local(): lax.all_gather(value_shard, 'fs', axis=0, tiled=True)  40.3 us
    psum x1, blocking collectives, local(): all_squares = lax.psum(squares, ('fs', 'tp'))  39.4 us
    psum x1, blocking collectives, local(): lax.psum(value_right_part.astype(jnp.bfloat16), 'fs').astype(jnp.float32)  36.9 us
    psum x1, waiting for transfers between devices, local(): lax.psum(query_left_part.astype(jnp.bfloat16), 'tp').astype(jnp.float32)  34.4 us
    dot_general x1, matrix products, token_sum(): lax.dot_general(inputs, cotangent, (((0,), (0,)), ((), ())), preferred_el...  21.4 us
    psum x1, waiting for transfers between devices, local(): lax.psum(query_right_part.astype(jnp.bfloat16), 'fs').astype(jnp.float32)  19.2 us
  transfers between devices with their start and end apart: 5, of which 5 were waited for; matrix products, arithmetic and copies ran while one was open for 3% of the time, Pallas kernels for 0%

commit v1 on v0

v1 whole, which is shorter than its diff:
```python
import functools

import jax
import jax.numpy as jnp
from jax import lax
from jax.experimental import pallas as pl
from jax.experimental.pallas import tpu as pltpu
from jax.sharding import PartitionSpec as P

MESH = pl.DeviceIdType.MESH
f32 = jnp.float32
bf16 = jnp.bfloat16

momentum_decay = 0.9
statistic_decay = 0.9
learning_rate = 0.002
epsilon = 1e-06


def grid_of(fs):
    nz = 4 if fs % 4 == 0 else 1
    return nz, fs // nz


def greet(peers):
    barrier = pltpu.get_barrier_semaphore()
    for peer in peers:
        pl.semaphore_signal(barrier, inc=1, device_id=peer, device_id_type=MESH)
    pl.semaphore_wait(barrier, len(peers))


def remote(src, dst, send_sem, recv_sem, peer):
    return pltpu.make_async_remote_copy(
        src_ref=src,
        dst_ref=dst,
        send_sem=send_sem,
        recv_sem=recv_sem,
        device_id=peer,
        device_id_type=MESH,
    )


def mix(moment, gradient):
    return momentum_decay * moment + (1.0 - momentum_decay) * gradient


def gradient_kernel(
    nz,
    ny,
    cot_ref,
    x_ref,
    out_ref,
    xbuf,
    far,
    far_in,
    near,
    hop,
    hop_in,
    x_sem,
    y_send,
    y_recv,
    z_send,
    z_recv,
):
    me, tp = lax.axis_index("fs"), lax.axis_index("tp")
    z, y = me // ny, me % ny
    rows = out_ref.shape[1]
    chunks, far_count = nz * ny, nz * (ny - 1)
    slots = xbuf.shape[0]

    def owner(i):
        return ((z + i % nz + 1) % nz) * ny + (y + i // nz + 1) % ny

    def fetch(i):
        columns = pl.ds(pl.multiple_of(owner(i) * rows, 128), rows)
        return pltpu.make_async_copy(
            x_ref.at[:, columns], xbuf.at[i % slots], x_sem.at[i % slots]
        )

    def y_copy(i):
        peer = (z * ny + (y + i // nz + 1) % ny, tp)
        return remote(far.at[i], far_in.at[i], y_send.at[i], y_recv.at[i], peer)

    def z_copy(k):
        peer = (((z + k + 1) % nz) * ny + y, tp)
        return remote(hop.at[k], hop_in.at[k], z_send.at[k], z_recv.at[k], peer)

    for i in range(slots - 1):
        fetch(i).start()
    peers = [(z * ny + (y + d) % ny, tp) for d in range(1, ny)]
    peers += [(((z + d) % nz) * ny + y, tp) for d in range(1, nz)]
    greet(peers)

    width = min(rows, 256)

    def multiply(i, keep):
        @pl.when(i + slots - 1 < chunks)
        def _():
            fetch(i + slots - 1).start()

        fetch(i).wait()
        for j in range(rows // width):
            part = jnp.dot(
                cot_ref[...],
                xbuf[i % slots, :, j * width : (j + 1) * width],
                preferred_element_type=f32,
            )
            keep(i, slice(j * width, (j + 1) * width), part)

    def far_step(i, carry):
        def keep(i, columns, part):
            far[i, :, columns] = part.astype(bf16)

        multiply(i, keep)
        y_copy(i).start()
        return carry

    def near_step(i, carry):
        def keep(i, columns, part):
            near[i - far_count, :, columns] = part

        multiply(i, keep)
        return carry

    lax.fori_loop(0, far_count, far_step, 0)
    lax.fori_loop(far_count, chunks, near_step, 0)

    for k in range(nz):
        for d in range(ny - 1):
            y_copy(d * nz + k).wait_recv()
        total = near[k]
        for d in range(ny - 1):
            total = total + far_in[d * nz + k].astype(f32)
        if k < nz - 1:
            hop[k] = total.astype(bf16)
            z_copy(k).start()
        else:
            out_ref[...] = total
    for k in range(nz - 1):
        z_copy(k).wait_recv()
        out_ref[...] += hop_in[k].astype(f32)
    for i in range(far_count):
        y_copy(i).wait_send()
    for k in range(nz - 1):
        z_copy(k).wait_send()


def gradients_of_rows(nz, ny, cotangent, layer_input):
    columns, tokens = cotangent.shape
    rows = layer_input.shape[1] // (nz * ny)
    far_count = nz * (ny - 1)
    return pl.pallas_call(
        functools.partial(gradient_kernel, nz, ny),
        out_shape=jax.ShapeDtypeStruct((columns, rows), f32),
        in_specs=[
            pl.BlockSpec(memory_space=pltpu.VMEM),
            pl.BlockSpec(memory_space=pl.ANY),
        ],
        out_specs=pl.BlockSpec(memory_space=pltpu.VMEM),
        scratch_shapes=[
            pltpu.VMEM((3, tokens, rows), bf16),
            pltpu.VMEM((far_count, columns, rows), bf16),
            pltpu.VMEM((far_count, columns, rows), bf16),
            pltpu.VMEM((nz, columns, rows), f32),
            pltpu.VMEM((nz - 1, columns, rows), bf16),
            pltpu.VMEM((nz - 1, columns, rows), bf16),
            pltpu.SemaphoreType.DMA((3,)),
            pltpu.SemaphoreType.DMA((far_count,)),
            pltpu.SemaphoreType.DMA((far_count,)),
            pltpu.SemaphoreType.DMA((nz - 1,)),
            pltpu.SemaphoreType.DMA((nz - 1,)),
        ],
        compiler_params=pltpu.CompilerParams(collective_id=0, has_side_effects=True),
    )(cotangent, layer_input)


def dot_split(left, right, split_left):
    wide = left if split_left else right
    high = wide.astype(bf16)
    low = (wide - high.astype(f32)).astype(bf16)
    if split_left:
        return jnp.dot(high, right, preferred_element_type=f32) + jnp.dot(
            low, right, preferred_element_type=f32
        )
    return jnp.dot(left, high, preferred_element_type=f32) + jnp.dot(
        left, low, preferred_element_type=f32
    )


def outer(a):
    return lax.dot_general(a, a, (((1,), (1,)), ((), ())), preferred_element_type=f32)


def total_of(x):
    return jnp.sum(jnp.sum(x, axis=0, keepdims=True), axis=1, keepdims=True)


def update_kernel(
    nz,
    ny,
    ntp,
    grad_ref,
    weight_q,
    weight_v,
    moment_q,
    moment_v,
    left_stat_q,
    left_stat_v,
    right_stat_q,
    right_stat_v,
    left_root_q,
    left_root_v,
    right_root_q,
    right_root_v,
    update_q,
    update_v,
    moment_new_q,
    moment_new_v,
    left_new_q,
    left_new_v,
    right_new_q,
    right_new_v,
    copy_q,
    copy_v,
    left_terms,
    right_terms,
    tp_squares,
    fs_squares,
    tp_sems,
    fs_sems,
    left_sems,
    right_sems,
    z_sems,
    y_sems,
):
    nfs = nz * ny
    me, tp = lax.axis_index("fs"), lax.axis_index("tp")
    z, y = me // ny, me % ny
    rows, width_q = moment_q.shape
    width_v = moment_v.shape[1]
    blocks, block = left_root_q.shape[:2]
    head = right_stat_q.shape[1]
    heads_q, heads_v = right_stat_q.shape[0], right_stat_v.shape[0]

    tp_peers = [(me, (tp + d) % ntp) for d in range(1, ntp)]
    fs_peers = [((me + d) % nfs, tp) for d in range(1, nfs)]

    def direction(grad, moment, moment_new, left_root, right_root, update):
        new = mix(moment[...], grad)
        moment_new[...] = new
        turned = dot_split(new, right_root[...], True)
        squares = jnp.zeros((1, 1), f32)
        for b in range(blocks):
            part = dot_split(left_root[b], turned[b * block : (b + 1) * block], False)
            update[b * block : (b + 1) * block, :] = part
            squares = squares + total_of(part * part)
        return total_of(new * new), squares

    grad_q = grad_ref[:width_q, :].T
    grad_v = grad_ref[width_q:, :].T
    sums = direction(grad_q, moment_q, moment_new_q, left_root_q, right_root_q, update_q)
    sums += direction(grad_v, moment_v, moment_new_v, left_root_v, right_root_v, update_v)
    row = lax.broadcasted_iota(jnp.int32, (8, 128), 0)
    tile = jnp.zeros((8, 128), f32)
    for i, one in enumerate(sums):
        tile = jnp.where(row == i, one, tile)
    tp_squares[tp] = tile

    greet(tp_peers + fs_peers)

    def spread(buffer, own, sems, peers):
        return [
            remote(buffer.at[own], buffer.at[own], sems.at[0, d], sems.at[1, d], peer)
            for d, peer in enumerate(peers)
        ]

    tp_copies = spread(tp_squares, tp, tp_sems, tp_peers)
    fs_copies = spread(fs_squares, me, fs_sems, fs_peers)
    left_copies = spread(left_terms, tp, left_sems, tp_peers)
    right_copies = spread(right_terms, me, right_sems, fs_peers)

    for copy in tp_copies:
        copy.start()
    for grad, first in ((grad_q, 0), (grad_v, blocks)):
        narrow = grad.astype(bf16)
        for b in range(blocks):
            left_terms[tp, first + b] = outer(narrow[b * block : (b + 1) * block]).astype(bf16)
    for h in range(heads_q + heads_v):
        right_terms[me, h] = outer(grad_ref[h * head : (h + 1) * head, :].astype(bf16)).astype(bf16)
    for copy in tp_copies:
        copy.wait_recv()
    tile = tp_squares[0]
    for i in range(1, ntp):
        tile = tile + tp_squares[i]
    fs_squares[me] = tile
    for copy in fs_copies + left_copies + right_copies:
        copy.start()
    for copy in fs_copies:
        copy.wait_recv()
    tile = fs_squares[0]
    for i in range(1, nfs):
        tile = tile + fs_squares[i]

    own_rows = pl.ds(pl.multiple_of(me * rows, rows), rows)
    for i, (update, weight, copy) in enumerate(
        ((update_q, weight_q, copy_q), (update_v, weight_v, copy_v))
    ):
        scale = jnp.sqrt(
            tile[2 * i : 2 * i + 1, :1] / (tile[2 * i + 1 : 2 * i + 2, :1] + epsilon)
        )
        scaled = scale * update[...]
        update[...] = scaled
        copy[own_rows, :] = (weight[...] - learning_rate * scaled).astype(bf16)

    def rows_of(device):
        return pl.ds(pl.multiple_of(device * rows, rows), rows)

    def z_copies(k):
        where = rows_of(me)
        peer = (((z + k) % nz) * ny + y, tp)
        return [
            remote(c.at[where, :], c.at[where, :], z_sems.at[0, i, k - 1], z_sems.at[1, i, k - 1], peer)
            for i, c in enumerate((copy_q, copy_v))
        ]

    def y_copies(d, k):
        where = rows_of(((z + nz - k) % nz) * ny + y)
        peer = (z * ny + (y + d) % ny, tp)
        n = (d - 1) * nz + k
        return [
            remote(c.at[where, :], c.at[where, :], y_sems.at[0, i, n], y_sems.at[1, i, n], peer)
            for i, c in enumerate((copy_q, copy_v))
        ]

    order = sorted(range(1, nz), key=lambda k: min(k, nz - k))
    for k in order:
        for copy in z_copies(k):
            copy.start()
    for d in range(1, ny):
        for copy in y_copies(d, 0):
            copy.start()

    for copy in left_copies + right_copies:
        copy.wait_recv()

    def add_up(terms, count, picked):
        total = terms[0, picked].astype(f32)
        for i in range(1, count):
            total = total + terms[i, picked].astype(f32)
        return total

    for new, stat, first, columns in (
        (left_new_q, left_stat_q, 0, width_q * ntp),
        (left_new_v, left_stat_v, blocks, width_v * ntp),
    ):
        for b in range(blocks):
            total = add_up(left_terms, ntp, first + b)
            new[b] = statistic_decay * stat[b] + (1.0 - statistic_decay) / columns * total
    for new, stat, first in ((right_new_q, right_stat_q, 0), (right_new_v, right_stat_v, heads_q)):
        for h in range(stat.shape[0]):
            total = add_up(right_terms, nfs, first + h)
            new[h] = statistic_decay * stat[h] + (1.0 - statistic_decay) / (rows * nfs) * total

    for k in order:
        for copy in z_copies(k):
            copy.wait_recv()
        for d in range(1, ny):
            for copy in y_copies(d, k):
                copy.start()
    for d in range(1, ny):
        for k in range(nz):
            for copy in y_copies(d, k):
                copy.wait()
    for k in order:
        for copy in z_copies(k):
            copy.wait_send()
    for copy in tp_copies + fs_copies + left_copies + right_copies:
        copy.wait_send()


def block_diagonal(root):
    count, head = root.shape[:2]
    same = jnp.arange(count)[:, None, None, None] == jnp.arange(count)[None, None, :, None]
    return jnp.where(same, root[:, :, None, :], 0).reshape(count * head, count * head)


def local(
    nfs,
    ntp,
    layer_input,
    query_cotangent,
    value_cotangent,
    query_weight,
    value_weight,
    query_moment,
    value_moment,
    query_left_stat,
    value_left_stat,
    query_right_stat,
    value_right_stat,
    query_left_root,
    value_left_root,
    query_right_root,
    value_right_root,
):
    nz, ny = grid_of(nfs)
    cotangent = jnp.concatenate([query_cotangent.T, value_cotangent.T], axis=0)
    gradient = gradients_of_rows(nz, ny, cotangent, layer_input)
    rows, width_q = query_weight.shape
    width_v = value_weight.shape[1]
    left_shape, right_q, right_v = query_left_stat.shape, query_right_stat.shape, value_right_stat.shape
    head_count = right_q[0] + right_v[0]
    shape = jax.ShapeDtypeStruct
    dma = pltpu.SemaphoreType.DMA
    vmem = pl.BlockSpec(memory_space=pltpu.VMEM)
    return pl.pallas_call(
        functools.partial(update_kernel, nz, ny, ntp),
        out_shape=(
            shape((rows, width_q), f32),
            shape((rows, width_v), f32),
            shape((rows, width_q), f32),
            shape((rows, width_v), f32),
            shape(left_shape, f32),
            shape(left_shape, f32),
            shape(right_q, f32),
            shape(right_v, f32),
            shape((rows * nfs, width_q), bf16),
            shape((rows * nfs, width_v), bf16),
        ),
        in_specs=[vmem] * 13,
        out_specs=(vmem,) * 10,
        scratch_shapes=[
            pltpu.VMEM((ntp, 2 * left_shape[0]) + left_shape[1:], bf16),
            pltpu.VMEM((nfs, head_count) + right_q[1:], bf16),
            pltpu.VMEM((ntp, 8, 128), f32),
            pltpu.VMEM((nfs, 8, 128), f32),
            dma((2, ntp - 1)),
            dma((2, nfs - 1)),
            dma((2, ntp - 1)),
            dma((2, nfs - 1)),
            dma((2, 2, nz - 1)),
            dma((2, 2, (ny - 1) * nz)),
        ],
        compiler_params=pltpu.CompilerParams(collective_id=1, has_side_effects=True),
    )(
        gradient,
        query_weight,
        value_weight,
        query_moment,
        value_moment,
        query_left_stat,
        value_left_stat,
        query_right_stat,
        value_right_stat,
        query_left_root,
        value_left_root,
        block_diagonal(query_right_root),
        block_diagonal(value_right_root),
    )


def solution(mesh):
    matrix, left, right = P("fs", "tp"), P("fs", None, None), P("tp", None, None)
    return jax.shard_map(
        functools.partial(local, mesh.shape["fs"], mesh.shape["tp"]),
        mesh=mesh,
        in_specs=(P("fs", None),) + (matrix,) * 6 + (left, left, right, right) * 2,
        out_specs=(matrix,) * 4 + (left, left, right, right) + (P(None, "tp"),) * 2,
        check_vma=False,
    )
```

time: 514 us -> 234 us (0.46)
  the two profiles are of different devices: /device:TPU:0 before, /device:TPU:16 now
where the time goes in v1:
time: 234 us
  Pallas kernels  211 us (90%)
  local copies, waits for them, and re-layouts  18.3 us (8%)
  other arithmetic  3.88 us (2%)
    pallas_call x1, Pallas kernels, local(): pl.pallas_call(functools.partial(update_kernel, nz, ny, ntp), out_shape=(...  131 us
    pallas_call x1, Pallas kernels, gradients_of_rows(): pl.pallas_call(functools.partial(gradient_kernel, nz, ny), out_shape=jax....  80 us
    unnamed x28, local copies, waits for them, and re-layouts  16.1 us

profile of v1, /device:TPU:16, one launch (start us, length us, event | category | flops | bytes accessed | tf_op | source)
XLA Modules:
  0.0 234.0 jit_solution(9088210065082672298)
XLA Ops:
  0.7 0.9 broadcast_select_fusion.1
  1.6 0.7 select_n.19.right_root_v
  2.3 1.3 copy.26
  3.6 1.1 broadcast_select_fusion
  4.7 1.4 select_n.17.right_root_q
  6.1 3.0 %copy.25 = bf16[2560,512]{0,1:T(8,128)(2,1)S(1)} copy(bf16[2560,512]{1,0:T(8,128)(2,1)} %param.16) | data formatting | bytes 5242880 | tf_op args[1]
  9.1 1.9 pad_maximum_fusion.cot_ref
  11.0 80.0 %shard_map.222.grad_ref = f32[640,512]{1,0:T(8,128)} custom-call(bf16[640,2560]{1,0:T(8,128)(2,1)} %pad_maximum_fusion.cot_ref, bf16[2560,4096]{1,0:T(8,128)(2,1)} %x_ref.1), custom_call_target="tpu_custom_call" | custom-call | tf_op jit(solution)/shard_map/pallas_call | solution.py:152
  91.0 131.1 %shard_map.223 = (f32[512,512]{1,0:T(8,128)}, f32[512,128]{1,0:T(8,128)}, f32[512,512]{1,0:T(8,128)}, f32[512,128]{1,0:T(8,128)}, f32[2,256,256]{2,1,0:T(8,128)}...) custom-call(f32[640,512]{1,0:T(8,128)} %shard_map.222.grad_ref, ...), custom_call_target="tpu_custom_call" | custom-call | tf_op jit(solution)/shard_map/pallas_call | solution.py:416
  222.1 0.0 copy-start.2
  222.1 0.0 copy-start.6
  222.1 0.0 copy-start.4
  222.1 0.0 copy-start.3
  222.2 0.0 copy-start.5
  222.2 2.4 %copy.37 = f32[512,512]{1,0:T(8,128)} copy(f32[512,512]{1,0:T(8,128)} %get-tuple-element.20) | data formatting | bytes 2097152
  224.6 0.0 copy-start.7
  224.6 0.0 copy-start
  224.6 1.8 copy.38
  226.4 0.0 copy-done.2
  226.4 1.0 copy.39
  227.4 0.0 copy-done.6
  227.4 0.7 copy.40
  228.1 0.0 copy-done.4
  228.1 0.8 copy.41
  228.9 0.0 copy-done.3
  228.9 0.8 copy.42
  229.7 0.0 copy-done.5
  229.7 0.7 copy.43
  230.4 0.0 copy-done.7
  230.4 0.6 copy.44
  231.0 0.0 copy-done
  231.0 0.0 copy-start.1
  231.0 2.0 copy.45
  233.0 0.0 copy-done.1
  233.0 1.0 copy.46
  (2 shorter events, 0.0 us)
Async XLA Ops:
  222.1 4.3 %copy-start.2 = (f32[512,512]{1,0:T(8,128)S(1)}, f32[512,512]{1,0:T(8,128)}, u32[]{:S(2)}) copy-start(f32[512,512]{1,0:T(8,128)} %get-tuple-element.22) | copy-start | bytes 3145732
  222.1 5.3 %copy-start.6 = (f32[512,128]{1,0:T(8,128)S(1)}, f32[512,128]{1,0:T(8,128)}, u32[]{:S(2)}) copy-start(f32[512,128]{1,0:T(8,128)} %get-tuple-element.23) | copy-start | bytes 786436
  222.1 5.9 %copy-start.4 = (f32[2,256,256]{2,1,0:T(8,128)S(1)}, f32[2,256,256]{2,1,0:T(8,128)}, u32[]{:S(2)}) copy-start(f32[2,256,256]{2,1,0:T(8,128)} %get-tuple-element.24) | copy-start | bytes 1572868
  222.1 6.7 %copy-start.3 = (f32[2,256,256]{2,1,0:T(8,128)S(1)}, f32[2,256,256]{2,1,0:T(8,128)}, u32[]{:S(2)}) copy-start(f32[2,256,256]{2,1,0:T(8,128)} %get-tuple-element.25) | copy-start | bytes 1572868
  222.2 7.5 %copy-start.5 = (f32[8,64,64]{2,1,0:T(8,128)S(1)}, f32[8,64,64]{2,1,0:T(8,128)}, u32[]{:S(2)}) copy-start(f32[8,64,64]{2,1,0:T(8,128)} %get-tuple-element.26) | copy-start | bytes 393220
  224.6 5.8 %copy-start.7 = (f32[2,64,64]{2,1,0:T(8,128)S(1)}, f32[2,64,64]{2,1,0:T(8,128)}, u32[]{:S(2)}) copy-start(f32[2,64,64]{2,1,0:T(8,128)} %get-tuple-element.27) | copy-start | bytes 98308
  224.6 6.4 %copy-start = (bf16[4096,512]{1,0:T(8,128)(2,1)S(1)}, bf16[4096,512]{1,0:T(8,128)(2,1)}, u32[]{:S(2)}) copy-start(bf16[4096,512]{1,0:T(8,128)(2,1)} %get-tuple-element.28) | copy-start | bytes 12582916
  231.0 2.0 copy-start.1

commit v2 on v1

--- a/solution.py
+++ b/solution.py
@@ -293,7 +293,7 @@
     for i in range(1, ntp):
         tile = tile + tp_squares[i]
     fs_squares[me] = tile
-    for copy in fs_copies + left_copies + right_copies:
+    for copy in fs_copies + left_copies:
         copy.start()
     for copy in fs_copies:
         copy.wait_recv()
@@ -340,6 +340,14 @@
         for copy in y_copies(d, 0):
             copy.start()
 
+    for copy in right_copies:
+        copy.start()
+    for k in order:
+        for copy in z_copies(k):
+            copy.wait_recv()
+        for d in range(1, ny):
+            for copy in y_copies(d, k):
+                copy.start()
     for copy in left_copies + right_copies:
         copy.wait_recv()
 
@@ -361,12 +369,6 @@
             total = add_up(right_terms, nfs, first + h)
             new[h] = statistic_decay * stat[h] + (1.0 - statistic_decay) / (rows * nfs) * total
 
-    for k in order:
-        for copy in z_copies(k):
-            copy.wait_recv()
-        for d in range(1, ny):
-            for copy in y_copies(d, k):
-                copy.start()
     for d in range(1, ny):
         for k in range(nz):
             for copy in y_copies(d, k):

time: 234 us -> 214 us (0.915)
  the two profiles are of different devices: /device:TPU:16 before, /device:TPU:0 now
where the time goes in v2:
time: 214 us
  Pallas kernels  191 us (89%)
  local copies, waits for them, and re-layouts  18.3 us (9%)
  other arithmetic  3.88 us (2%)
    pallas_call x1, Pallas kernels, local(): pl.pallas_call(functools.partial(update_kernel, nz, ny, ntp), out_shape=(...  108 us
    pallas_call x1, Pallas kernels, gradients_of_rows(): pl.pallas_call(functools.partial(gradient_kernel, nz, ny), out_shape=jax....  82.8 us
    unnamed x28, local copies, waits for them, and re-layouts  16.1 us

profile of v2, /device:TPU:0, one launch (start us, length us, event | category | flops | bytes accessed | tf_op | source)
XLA Modules:
  0.0 214.0 jit_solution(16125840531908250952)
XLA Ops:
  0.7 0.9 broadcast_select_fusion.1
  1.6 0.7 select_n.19.right_root_v
  2.3 1.3 copy.26
  3.6 1.1 broadcast_select_fusion
  4.7 1.4 select_n.17.right_root_q
  6.1 3.0 %copy.25 = bf16[2560,512]{0,1:T(8,128)(2,1)S(1)} copy(bf16[2560,512]{1,0:T(8,128)(2,1)} %param.16) | data formatting | bytes 5242880 | tf_op args[1]
  9.1 1.9 pad_maximum_fusion.cot_ref
  11.0 82.8 %shard_map.222.grad_ref = f32[640,512]{1,0:T(8,128)} custom-call(bf16[640,2560]{1,0:T(8,128)(2,1)} %pad_maximum_fusion.cot_ref, bf16[2560,4096]{1,0:T(8,128)(2,1)} %x_ref.1), custom_call_target="tpu_custom_call" | custom-call | tf_op jit(solution)/shard_map/pallas_call | solution.py:152
  93.7 108.4 %shard_map.223 = (f32[512,512]{1,0:T(8,128)}, f32[512,128]{1,0:T(8,128)}, f32[512,512]{1,0:T(8,128)}, f32[512,128]{1,0:T(8,128)}, f32[2,256,256]{2,1,0:T(8,128)}...) custom-call(f32[640,512]{1,0:T(8,128)} %shard_map.222.grad_ref, ...), custom_call_target="tpu_custom_call" | custom-call | tf_op jit(solution)/shard_map/pallas_call | solution.py:418
  202.2 0.0 copy-start.2
  202.2 0.0 copy-start.6
  202.2 0.0 copy-start.4
  202.2 0.0 copy-start.3
  202.2 0.0 copy-start.5
  202.2 2.4 %copy.37 = f32[512,512]{1,0:T(8,128)} copy(f32[512,512]{1,0:T(8,128)} %get-tuple-element.20) | data formatting | bytes 2097152
  204.6 0.0 copy-start.7
  204.6 0.0 copy-start
  204.6 1.8 copy.38
  206.4 0.0 copy-done.2
  206.4 1.0 copy.39
  207.4 0.0 copy-done.6
  207.4 0.7 copy.40
  208.1 0.0 copy-done.4
  208.1 0.8 copy.41
  208.9 0.0 copy-done.3
  208.9 0.8 copy.42
  209.7 0.0 copy-done.5
  209.7 0.7 copy.43
  210.4 0.0 copy-done.7
  210.4 0.6 copy.44
  211.1 0.0 copy-done
  211.1 0.0 copy-start.1
  211.1 2.0 copy.45
  213.1 0.0 copy-done.1
  213.1 1.0 copy.46
  (2 shorter events, 0.0 us)
Async XLA Ops:
  202.2 4.3 %copy-start.2 = (f32[512,512]{1,0:T(8,128)S(1)}, f32[512,512]{1,0:T(8,128)}, u32[]{:S(2)}) copy-start(f32[512,512]{1,0:T(8,128)} %get-tuple-element.22) | copy-start | bytes 3145732
  202.2 5.3 %copy-start.6 = (f32[512,128]{1,0:T(8,128)S(1)}, f32[512,128]{1,0:T(8,128)}, u32[]{:S(2)}) copy-start(f32[512,128]{1,0:T(8,128)} %get-tuple-element.23) | copy-start | bytes 786436
  202.2 5.9 %copy-start.4 = (f32[2,256,256]{2,1,0:T(8,128)S(1)}, f32[2,256,256]{2,1,0:T(8,128)}, u32[]{:S(2)}) copy-start(f32[2,256,256]{2,1,0:T(8,128)} %get-tuple-element.24) | copy-start | bytes 1572868
  202.2 6.7 %copy-start.3 = (f32[2,256,256]{2,1,0:T(8,128)S(1)}, f32[2,256,256]{2,1,0:T(8,128)}, u32[]{:S(2)}) copy-start(f32[2,256,256]{2,1,0:T(8,128)} %get-tuple-element.25) | copy-start | bytes 1572868
  202.2 7.5 %copy-start.5 = (f32[8,64,64]{2,1,0:T(8,128)S(1)}, f32[8,64,64]{2,1,0:T(8,128)}, u32[]{:S(2)}) copy-start(f32[8,64,64]{2,1,0:T(8,128)} %get-tuple-element.26) | copy-start | bytes 393220
  204.6 5.8 %copy-start.7 = (f32[2,64,64]{2,1,0:T(8,128)S(1)}, f32[2,64,64]{2,1,0:T(8,128)}, u32[]{:S(2)}) copy-start(f32[2,64,64]{2,1,0:T(8,128)} %get-tuple-element.27) | copy-start | bytes 98308
  204.6 6.4 %copy-start = (bf16[4096,512]{1,0:T(8,128)(2,1)S(1)}, bf16[4096,512]{1,0:T(8,128)(2,1)}, u32[]{:S(2)}) copy-start(bf16[4096,512]{1,0:T(8,128)(2,1)} %get-tuple-element.28) | copy-start | bytes 12582916
  211.1 2.0 copy-start.1
